TPU v7x, 32 devices: a whole 2x2x4 slice. The times are simulated.
32 devices in a mesh: ep: 8 (over z, y), tp: 4 (over x, core).
Axes of the slice: x: 2, y: 2, z: 4, core: 2. Of those that a mesh axis runs over, the one named last changes fastest.
Arguments:
- queries: bfloat16 [1536, 2048], P('ep', 'tp'), may hold values from -8 to 8
- keys: bfloat16 [1536, 512], P('ep', 'tp'), may hold values from -8 to 8
- values: bfloat16 [1536, 512], P('ep', 'tp'), may hold values from -6 to 6
- query_gain: float32 [2048], P('tp'), may hold values from 0.5 to 6
- key_gain: float32 [512], P('tp'), may hold values from 0.7 to 6
- out_weight: bfloat16 [2048, 4096], P('tp'), may hold values from -0.125 to 0.125
- expert_input: bfloat16 [2048, 4096], P(('ep', 'tp')), may hold values from -6 to 6
- norm_gain: float32 [4096], replicated, may hold values from 0.1 to 1.9
- routes: int32 [2048, 2], P(('ep', 'tp')), may hold values from 0 to 7, all different within a row; in each aligned block of 64 rows (0 to 63, 64 to 127, ...) at most 32 rows name the same one
- route_weight: float32 [2048, 2], P(('ep', 'tp')), may hold values from 0.2 to 2
- gate_weight: bfloat16 [8, 4096, 1024], P('ep', None, 'tp'), may hold values from -0.09375 to 0.09375
- up_weight: bfloat16 [8, 4096, 1024], P('ep', None, 'tp'), may hold values from -0.09375 to 0.09375
- down_weight: bfloat16 [8, 1024, 4096], P('ep', 'tp'), may hold values from -0.1875 to 0.1875
Outputs:
- mixed: bfloat16 [1536, 4096], P(('ep', 'tp'))
- moe_out: bfloat16 [2048, 4096], P(('ep', 'tp'))
Inputs may be any that keep to these rules, and one draw needn't show every extreme that they name: `routes`: each row names 2 different experts; in the rows of one device no expert is named by more than 32 rows, and in some device one expert is named by exactly 32 rows.
All inputs are finite; a program needn't handle non-finite values.
Results may differ from a plain program's by a relative error of at most 0.013.
The roundings to bfloat16 on the way count: a program that leaves them out, or rounds other values in their place, can miss the bound.
Values may be sent and summed in bfloat16 or wider, within the bound.
A program may use at most 128 MiB of HBM per device.

v0:
```python
import jax
import jax.numpy as jnp
from jax import lax
from jax.sharding import PartitionSpec as P

HEAD_DIM = 64
GRID_W = 128


NORM_EPS = 1e-06
ROPE_BASE = 10000.0


def rotate(vectors, grid_rows, grid_cols):
    quarter = vectors.shape[-1] // 4
    inverse = ROPE_BASE ** (-jnp.arange(quarter, dtype=jnp.float32) / quarter)
    angle_row = grid_rows[:, None] * inverse
    angle_col = grid_cols[:, None] * inverse
    angles = jnp.concatenate([angle_row, angle_row, angle_col, angle_col], axis=-1)[:, None, :]
    part_one, part_two, part_three, part_four = jnp.split(vectors, 4, axis=-1)
    turned = jnp.concatenate([-part_two, part_one, -part_four, part_three], axis=-1)
    return vectors * jnp.cos(angles) + turned * jnp.sin(angles)


def head_norm(raw_rows, gains, head_count, offset):
    row_count = raw_rows.shape[0]
    flat_rows = raw_rows.astype(jnp.float32).reshape(row_count, head_count, -1)
    unit_vec = flat_rows * lax.rsqrt(
        jnp.mean(flat_rows * flat_rows, axis=-1, keepdims=True) + NORM_EPS
    )
    unit_vec = unit_vec * gains.reshape(head_count, -1)
    places = offset + jnp.arange(row_count, dtype=jnp.int32)
    grid_rows = (places // GRID_W).astype(jnp.float32)
    grid_cols = (places % GRID_W).astype(jnp.float32)
    return rotate(unit_vec, grid_rows, grid_cols).astype(jnp.bfloat16).reshape(row_count, -1)


def absorb(running, key_block, value_block, grouped, score_scale):
    run_max, weight_sum, summed = running
    kv_count = grouped.shape[1]
    key_heads = key_block.reshape(key_block.shape[0], kv_count, -1)
    value_heads = value_block.reshape(value_block.shape[0], kv_count, -1)
    scores = (
        jnp.einsum("qhgd,khd->hgqk", grouped, key_heads, preferred_element_type=jnp.float32)
        * score_scale
    )
    new_max = jnp.maximum(run_max, jnp.max(scores, axis=-1))
    rescale = jnp.exp(run_max - new_max)
    weights = jnp.exp(scores - new_max[..., None])
    weight_sum = weight_sum * rescale + jnp.sum(weights, axis=-1)
    update = jnp.einsum(
        "hgqk,khd->qhgd",
        weights.astype(jnp.bfloat16),
        value_heads,
        preferred_element_type=jnp.float32,
    )
    summed = summed * jnp.transpose(rescale, (2, 0, 1))[..., None] + update
    return (new_max, weight_sum, summed)


def run_experts(sending, gate_weight, up_weight, down_weight):
    arrived = lax.all_to_all(sending, "ep", split_axis=0, concat_axis=0, tiled=True)
    shard_rows = lax.all_gather(arrived, "tp", axis=0, tiled=True)
    gate_out = jnp.dot(shard_rows, gate_weight[0], preferred_element_type=jnp.float32)
    up_out = jnp.dot(shard_rows, up_weight[0], preferred_element_type=jnp.float32)
    hidden = (jax.nn.silu(gate_out) * up_out).astype(jnp.bfloat16)
    results = lax.psum_scatter(
        jnp.dot(hidden, down_weight[0], preferred_element_type=jnp.float32).astype(jnp.bfloat16),
        "tp",
        scatter_dimension=0,
        tiled=True,
    )
    return lax.all_to_all(results, "ep", split_axis=0, concat_axis=0, tiled=True)


def shards(
    queries,
    keys,
    values,
    query_gain,
    key_gain,
    out_weight,
    expert_input,
    norm_gain,
    routes,
    route_weight,
    gate_weight,
    up_weight,
    down_weight,
):
    tok_mix = queries.shape[0]
    head_count = query_gain.shape[0] // HEAD_DIM
    kv_count = key_gain.shape[0] // HEAD_DIM
    group_size = head_count // kv_count
    offset = lax.axis_index("ep") * tok_mix
    q_turned = head_norm(queries, query_gain, head_count, offset)
    k_turned = head_norm(keys, key_gain, kv_count, offset)
    grouped = q_turned.reshape(tok_mix, kv_count, group_size, HEAD_DIM)
    score_scale = HEAD_DIM ** (-0.5)
    start_state = (
        jnp.full((kv_count, group_size, tok_mix), -jnp.inf, jnp.float32),
        jnp.zeros((kv_count, group_size, tok_mix), jnp.float32),
        jnp.zeros((tok_mix, kv_count, group_size, HEAD_DIM), jnp.float32),
    )
    running = start_state
    key_piece = lax.all_gather(k_turned, "ep", axis=0, tiled=True)
    value_piece = lax.all_gather(values, "ep", axis=0, tiled=True)
    length = key_piece.shape[0]
    block_len = length
    while block_len > 2048 and block_len % 2 == 0:
        block_len = block_len // 2
    key_blocks = key_piece.reshape(length // block_len, block_len, key_piece.shape[1])
    value_blocks = value_piece.reshape(length // block_len, block_len, value_piece.shape[1])

    def advance(inner_state, key_value):
        return (absorb(inner_state, key_value[0], key_value[1], grouped, score_scale), None)

    running, unused = lax.scan(advance, running, (key_blocks, value_blocks))
    final_max, weight_sum, summed = running
    attended = (
        (summed / jnp.transpose(weight_sum, (2, 0, 1))[..., None])
        .reshape(tok_mix, -1)
        .astype(jnp.bfloat16)
    )
    mixed = lax.psum_scatter(
        jnp.dot(attended, out_weight, preferred_element_type=jnp.float32).astype(jnp.bfloat16),
        "tp",
        scatter_dimension=0,
        tiled=True,
    )
    tok_exp = expert_input.shape[0]
    top_count = routes.shape[1]
    expert_count = lax.axis_size("ep")
    capacity = 2 * top_count * tok_exp // expert_count
    as_float = expert_input.astype(jnp.float32)
    normed = (
        as_float
        * lax.rsqrt(jnp.mean(as_float * as_float, axis=-1, keepdims=True) + NORM_EPS)
        * norm_gain
    ).astype(jnp.bfloat16)
    flat_routes = routes.reshape(-1)
    route_hits = (
        flat_routes[:, None] == jnp.arange(expert_count, dtype=jnp.int32)[None, :]
    ).astype(jnp.int32)
    slot_rank = jnp.sum((jnp.cumsum(route_hits, axis=0) - route_hits) * route_hits, axis=1)
    slot_ids = flat_routes * capacity + slot_rank
    placed = jnp.arange(expert_count * capacity, dtype=jnp.int32)[:, None] == slot_ids[None, :]
    placed = jnp.any(placed.reshape(expert_count * capacity, tok_exp, top_count), axis=2).astype(
        jnp.bfloat16
    )
    outbound = jnp.dot(placed, normed, preferred_element_type=jnp.float32).astype(jnp.bfloat16)
    model_width = outbound.shape[1]
    half_cap = capacity // 2
    laid = outbound.reshape(expert_count, capacity, model_width)
    first_half = run_experts(
        laid[:, :half_cap].reshape(expert_count * half_cap, model_width),
        gate_weight,
        up_weight,
        down_weight,
    )
    second_half = run_experts(
        laid[:, half_cap:].reshape(expert_count * half_cap, model_width),
        gate_weight,
        up_weight,
        down_weight,
    )
    back_rows = jnp.concatenate(
        [
            first_half.reshape(expert_count, half_cap, model_width),
            second_half.reshape(expert_count, half_cap, model_width),
        ],
        axis=1,
    )
    back_rows = back_rows.reshape(expert_count * capacity, model_width)
    picked = back_rows[slot_ids.reshape(tok_exp, top_count)]
    moe_out = jnp.sum(picked.astype(jnp.float32) * route_weight[:, :, None], axis=1).astype(
        jnp.bfloat16
    )
    return (mixed, moe_out)


def solution(mesh):
    placed = (
        P("ep", "tp"),
        P("ep", "tp"),
        P("ep", "tp"),
        P("tp"),
        P("tp"),
        P("tp", None),
        P(("ep", "tp"), None),
        P(),
        P(("ep", "tp"), None),
        P(("ep", "tp"), None),
        P("ep", None, "tp"),
        P("ep", None, "tp"),
        P("ep", "tp", None),
    )
    return jax.shard_map(
        shards,
        mesh=mesh,
        in_specs=placed,
        out_specs=(P(("ep", "tp"), None), P(("ep", "tp"), None)),
        check_vma=False,
    )
```

profile of v0, /device:TPU:0, one launch (start us, length us, event | category | flops | bytes accessed | tf_op | source)
XLA Modules:
  0.0 270.8 jit_solution(8384005811426926461)
XLA Ops:
  7.2 0.9 copy.60
  8.1 0.1 eq.33
  8.3 0.1 fusion.72
  8.4 0.2 reduce_window_sum.11
  8.5 0.2 select_reduce_fusion
  8.7 0.1 reduce_sum.64
  8.9 1.2 compare_select_fusion
  10.2 0.1 fusion.71
  10.2 1.2 fusion.37
  11.5 1.8 convolution_convert_fusion.2
  13.3 0.2 fusion.82
  13.5 33.0 %all_to_all.36 = bf16[8,16,4096]{2,1,0:T(8,128)(2,1)} all-to-all(bf16[8,16,4096]{2,1,0:T(8,128)(2,1)S(1)} %get-tuple-element.20), channel_id=1, replica_groups=mesh['ep'=8,'tp'=4] {'ep'}, dimensions={0} | all-to-all | bytes 2097152 | tf_op jit(solution)/shard_map/all_to_all | solution.py:62
  46.6 29.0 %all_to_all.37 = bf16[8,16,4096]{2,1,0:T(8,128)(2,1)} all-to-all(bf16[8,16,4096]{2,1,0:T(8,128)(2,1)S(1)} %get-tuple-element.28), channel_id=1, replica_groups=mesh['ep'=8,'tp'=4] {'ep'}, dimensions={0} | all-to-all | bytes 2097152 | tf_op jit(solution)/shard_map/all_to_all | solution.py:62
  75.6 4.5 %all-gather.3.cloned.1.call-done = bf16[512,4096]{1,0:T(8,128)(2,1)} async-done(((bf16[128,4096]{1,0:T(8,128)(2,1)}), bf16[512,4096]{1,0:T(8,128)(2,1)}) %all-gather.3.cloned.1.call-update) | async-done | bytes 4194320 | tf_op jit(solution)/shard_map/all_gather | solution.py:63
  80.1 4.1 %fusion.13 = f32[512,256]{1,0:T(8,128)S(1)} fusion(bf16[512,4096]{1,0:T(8,128)(2,1)} %all-gather.3.cloned.1.call-done, bf16[1,4096,256]{2,1,0:T(8,128)(2,1)} %param.23), kind=kOutput, calls=%fused_computation.20 | convolution fusion | flops 1073741824 | bytes 6815744 | tf_op jit(solution)/shard_map/dot_general | solution.py:64
  84.3 9.4 %convolution_convert_fusion.1 = bf16[512,4096]{1,0:T(8,128)(2,1)} fusion(bf16[1,256,4096]{2,1,0:T(8,128)(2,1)S(1)} %copy-done, bf16[512,4096]{1,0:T(8,128)(2,1)} %all-gather.3.cloned.1.call-done, bf16[1,4096,256]{2,1,0:T(8,128)(2,1)} %param.24, f32[512,256]{1,0:T(8,128)S(1)} %fusion.13), kind=kOutput, calls=%fused_computation.7 | convolution fusion | flops 2150367232 | bytes 13107200 | tf_op jit(solution)/shard_map/dot_general | solution.py:68
  93.8 22.4 %all-gather.5.cloned.1.call-done = bf16[512,4096]{1,0:T(8,128)(2,1)} async-done(((bf16[128,4096]{1,0:T(8,128)(2,1)}), bf16[512,4096]{1,0:T(8,128)(2,1)}) %all-gather.5.cloned.1.call-update) | async-done | bytes 4194320 | tf_op jit(solution)/shard_map/all_gather | solution.py:63
  116.2 4.1 %fusion.11 = f32[512,256]{1,0:T(8,128)S(1)} fusion(bf16[512,4096]{1,0:T(8,128)(2,1)} %all-gather.5.cloned.1.call-done, bf16[1,4096,256]{2,1,0:T(8,128)(2,1)} %param.23), kind=kOutput, calls=%fused_computation.18 | convolution fusion | flops 1073741824 | bytes 6815744 | tf_op jit(solution)/shard_map/dot_general | solution.py:64
  120.3 9.3 %convolution_convert_fusion = bf16[512,4096]{1,0:T(8,128)(2,1)} fusion(bf16[1,256,4096]{2,1,0:T(8,128)(2,1)S(1)} %copy-done, bf16[512,4096]{1,0:T(8,128)(2,1)} %all-gather.5.cloned.1.call-done, bf16[1,4096,256]{2,1,0:T(8,128)(2,1)} %param.24, f32[512,256]{1,0:T(8,128)S(1)} %fusion.11), kind=kOutput, calls=%fused_computation.6 | convolution fusion | flops 2150367232 | bytes 13107200 | tf_op jit(solution)/shard_map/dot_general | solution.py:68
  129.6 0.6 copy-done.5
  130.4 0.1 copy.55
  130.6 0.1 mul.254
  130.7 0.1 fusion.74
  130.9 0.1 multiply_multiply_fusion.1
  131.1 0.1 fusion.69
  131.2 0.1 copy.56
  131.3 31.4 %all_gather.12 = bf16[1536,128]{1,0:T(8,128)(2,1)S(1)} all-gather(bf16[192,128]{1,0:T(8,128)(2,1)S(1)} %copy.56), channel_id=1, replica_groups=mesh['ep'=8,'tp'=4] {'ep'}, dimensions={0}, use_global_device_ids=true | all-gather | bytes 442368 | tf_op jit(solution)/shard_map/all_gather | solution.py:106
  162.6 0.2 copy.57
  162.8 0.1 copy.58
  163.1 0.1 multiply_multiply_fusion
  163.2 1.7 bitcast_reduce_fusion
  165.0 0.6 multiply_bitcast_fusion
  165.6 3.0 %copy-done.1 = f32[2,1536,192,4]{1,2,3,0:T(8,128)} copy-done((f32[2,1536,192,4]{1,2,3,0:T(8,128)}, f32[2,1536,192,4]{1,2,3,0:T(8,128)S(1)}, u32[]{:S(2)}) %copy-start.1) | copy-done | bytes 9437208
  168.6 1.7 fusion.1
  170.3 5.4 %all-to-all-start.1 = ((bf16[8,16,4096]{2,1,0:T(8,128)(2,1)}), bf16[8,16,4096]{2,1,0:T(8,128)(2,1)S(1)}, u32[]{:S(2)}, u32[]{:S(2)}) async-start(bf16[8,16,4096]{2,1,0:T(8,128)(2,1)} %bitcast.119), calls=%async_computation.3 | async-start | bytes 2097152 | tf_op jit(solution)/shard_map/all_to_all | solution.py:73
  175.8 41.5 %all_gather.13 = bf16[1536,128]{1,0:T(8,128)(2,1)S(1)} all-gather(bf16[192,128]{1,0:T(8,128)(2,1)} %param.15), channel_id=1, replica_groups=mesh['ep'=8,'tp'=4] {'ep'}, dimensions={0}, use_global_device_ids=true | all-gather | bytes 442368 | tf_op jit(solution)/shard_map/all_gather | solution.py:107
  217.3 0.9 copy.59
  218.3 5.8 %fusion.43 = bf16[192,2,4,64]{0,3,2,1:T(8,128)(2,1)S(1)} fusion(bf16[1536,2,64,1]{0,2,3,1:T(8,128)(2,1)} %bitcast.125, f32[2,1536,192,4]{1,2,3,0:T(8,128)} %copy-done.1, f32[2,4,192]{2,1,0:T(4,128)S(1)} %get-tuple-element.41, f32[192,2,4]{0,2,1:T(4,128)S(1)} %bitcast_add_fusion.1, f32[192,2,4]{0,2,1:T(4,128)} %multiply_bitcast_fusion), kind=kOutput, calls=%fused_computation.35 | convolution fusion | flops 309362688 | bytes 10045440 | tf_op jit(solution)/shard_map/while/body/eval_jaxpr/hgqk,khd->qhgd/dot_general | solution.py:51
  224.2 2.2 convolution_convert_fusion.3
  226.4 4.5 %all-to-all-start.3 = ((bf16[8,16,4096]{2,1,0:T(8,128)(2,1)}), bf16[8,16,4096]{2,1,0:T(8,128)(2,1)}, u32[]{:S(2)}, u32[]{:S(2)}) async-start(bf16[8,16,4096]{2,1,0:T(8,128)(2,1)} %bitcast.120), calls=%async_computation.6 | async-start | bytes 2097152 | tf_op jit(solution)/shard_map/all_to_all | solution.py:73
  230.9 0.1 copy.62
  231.0 0.1 reshape.276
  231.1 0.1 copy.63
  231.2 18.3 %all-to-all-done.3 = bf16[8,16,4096]{2,1,0:T(8,128)(2,1)} async-done(((bf16[8,16,4096]{2,1,0:T(8,128)(2,1)}), bf16[8,16,4096]{2,1,0:T(8,128)(2,1)}, u32[]{:S(2)}, u32[]{:S(2)}) %all-to-all-start.3) | async-done | bytes 1048608 | tf_op jit(solution)/shard_map/all_to_all | solution.py:73
  249.5 2.8 %pad_maximum_fusion = bf16[8,32,4096]{2,1,0:T(8,128)(2,1)} fusion(bf16[8,16,4096]{2,1,0:T(8,128)(2,1)} %all-to-all-done.3, bf16[8,16,4096]{2,1,0:T(8,128)(2,1)S(1)} %all-to-all-done.1), kind=kLoop, calls=%fused_computation.11 | loop fusion | flops 4194304 | bytes 4194304 | tf_op jit(solution)/shard_map/concatenate | solution.py:167
  252.3 4.1 %gather_fusion = bf16[128,4096]{1,0:T(8,128)(2,1)S(1)} fusion(bf16[256,4096]{1,0:T(8,128)(2,1)} %bitcast.113, s32[1024]{0:T(1024)S(1)} %pad_clamp_fusion), kind=kCustom, calls=%fused_computation | custom fusion | bytes 2097664 | tf_op jit(solution)/shard_map/gather | solution.py:175
  256.4 2.4 reshape.284
  258.7 5.6 %multiply_reduce_fusion = bf16[64,4096]{1,0:T(8,128)(2,1)} fusion(f32[64,2,4096]{2,1,0:T(2,128)} %reshape.284, f32[64,2]{1,0:T(8,128)S(1)} %copy.63), kind=kLoop, calls=%fused_computation.22 | loop fusion | flops 786432 | bytes 2621952 | tf_op jit(solution)/shard_map/reduce_sum | solution.py:176
  (47 shorter events, 0.9 us)
Async XLA Ops:
  7.2 77.1 %copy-start = (bf16[1,256,4096]{2,1,0:T(8,128)(2,1)S(1)}, bf16[1,256,4096]{2,1,0:T(8,128)(2,1)}, u32[]{:S(2)}) copy-start(bf16[1,256,4096]{2,1,0:T(8,128)(2,1)} %param.25) | copy-start | bytes 6291460
  7.2 73.0 %all-gather.3.cloned.1.call-start = ((), (), s32[]{:S(2)}) async-start(), calls=%async_computation.8 | async-start | bytes 5242880 | tf_op jit(solution)/shard_map/all_gather | solution.py:63
  46.5 69.7 %all-gather.5.cloned.1.call-start = ((), (), s32[]{:S(2)}) async-start(), calls=%async_computation.10 | async-start | bytes 5242880 | tf_op jit(solution)/shard_map/all_gather | solution.py:63
  75.5 94.8 %reduce-scatter.6.cloned.1.call-start = ((), (), s32[]{:S(2)}) async-start(), calls=%async_computation.9 | async-start | bytes 5242880 | tf_op jit(solution)/shard_map/reduce_scatter | solution.py:67
  93.7 132.7 %reduce-scatter.8.cloned.1.call-start = ((), (), s32[]{:S(2)}) async-start(), calls=%async_computation.11 | async-start | bytes 5242880 | tf_op jit(solution)/shard_map/reduce_scatter | solution.py:67
  129.6 0.7 copy-start.5
  129.6 0.8 copy-start.4
  129.6 1.0 copy-start.8
  129.6 33.2 %copy-start.3 = (bf16[192,512]{1,0:T(8,128)(2,1)S(1)}, bf16[192,512]{1,0:T(8,128)(2,1)}, u32[]{:S(2)}) copy-start(bf16[192,512]{1,0:T(8,128)(2,1)} %param.13) | copy-start | bytes 589828
  164.9 3.6 %copy-start.1 = (f32[2,1536,192,4]{1,2,3,0:T(8,128)}, f32[2,1536,192,4]{1,2,3,0:T(8,128)S(1)}, u32[]{:S(2)}) copy-start(f32[2,1536,192,4]{1,2,3,0:T(8,128)S(1)} %get-tuple-element.42) | copy-start | bytes 28311556
  170.3 56.1 %all-to-all-start.1 = ((bf16[8,16,4096]{2,1,0:T(8,128)(2,1)}), bf16[8,16,4096]{2,1,0:T(8,128)(2,1)S(1)}, u32[]{:S(2)}, u32[]{:S(2)}) async-start(bf16[8,16,4096]{2,1,0:T(8,128)(2,1)} %bitcast.119), calls=%async_computation.3 | async-start | bytes 2097152 | tf_op jit(solution)/shard_map/all_to_all | solution.py:73
  175.8 88.5 %reduce-scatter.4.cloned.1.call-start = ((), (), s32[]{:S(2)}) async-start(), calls=%async_computation.7 | async-start | bytes 1966080 | tf_op jit(solution)/shard_map/reduce_scatter | solution.py:125
  218.3 5.9 %copy-start.2 = (bf16[512,4096]{1,0:T(8,128)(2,1)S(1)}, bf16[512,4096]{1,0:T(8,128)(2,1)}, u32[]{:S(2)}) copy-start(bf16[512,4096]{1,0:T(8,128)(2,1)} %param.18) | copy-start | bytes 12582916
  224.1 6.7 %copy-start.6 = (s32[64,2]{0,1:T(2,128)S(1)}, s32[64,2]{0,1:T(2,128)}, u32[]{:S(2)}) copy-start(s32[64,2]{0,1:T(2,128)} %get-tuple-element.16) | copy-start | bytes 1540
  224.2 7.0 %copy-start.7 = (f32[64,2]{0,1:T(2,128)S(1)}, f32[64,2]{0,1:T(2,128)}, u32[]{:S(2)}) copy-start(f32[64,2]{0,1:T(2,128)} %param.22) | copy-start | bytes 1540
  226.4 23.1 %all-to-all-start.3 = ((bf16[8,16,4096]{2,1,0:T(8,128)(2,1)}), bf16[8,16,4096]{2,1,0:T(8,128)(2,1)}, u32[]{:S(2)}, u32[]{:S(2)}) async-start(bf16[8,16,4096]{2,1,0:T(8,128)(2,1)} %bitcast.120), calls=%async_computation.6 | async-start | bytes 2097152 | tf_op jit(solution)/shard_map/all_to_all | solution.py:73
Sparse Core Ops, SparseCore 0:
  46.6 33.4 all-gather.2
  81.7 34.4 all-gather.4
  118.7 44.5 reduce-scatter.5
  165.7 44.5 reduce-scatter.7
  226.5 26.4 reduce-scatter.3
where the time goes:
time: 271 us
  blocking collectives  135 us (50%)
  waiting for transfers between devices  45.4 us (17%)
  matrix products  38.4 us (14%)
  other arithmetic  14.4 us (5%)
  between operations  14.1 us (5%)
  local copies, waits for them, and re-layouts  13.5 us (5%)
  starting transfers between devices  10.1 us (4%)
    all_to_all x2, blocking collectives, run_experts(): lax.all_to_all(sending, 'ep', split_axis=0, concat_axis=0, tiled=True)  61.9 us
    all_gather x1, blocking collectives, shards(): value_piece = lax.all_gather(values, 'ep', axis=0, tiled=True)  41.5 us
    all_gather x1, blocking collectives, shards(): key_piece = lax.all_gather(k_turned, 'ep', axis=0, tiled=True)  31.4 us
    all_gather x2, waiting for transfers between devices, run_experts(): shard_rows = lax.all_gather(arrived, 'tp', axis=0, tiled=True)  27 us
    dot_general x2, matrix products, run_experts(): jnp.dot(hidden, down_weight[0], preferred_element_type=jnp.float32)  18.7 us
    all_to_all x2, waiting for transfers between devices, run_experts(): lax.all_to_all(results, 'ep', split_axis=0, concat_axis=0, tiled=True)  18.3 us
    all_to_all x2, starting transfers between devices, run_experts(): lax.all_to_all(results, 'ep', split_axis=0, concat_axis=0, tiled=True)  9.9 us
    dot_general x2, matrix products, run_experts(): jnp.dot(shard_rows, gate_weight[0], preferred_element_type=jnp.float32)  8.23 us
  transfers between devices with their start and end apart: 7, of which 3 were waited for; matrix products, arithmetic and copies ran while one was open for 21% of the time, Pallas kernels for 0%

commit v1 on v0

--- a/solution.py
+++ b/solution.py
@@ -1,6 +1,10 @@
+import functools
+
 import jax
 import jax.numpy as jnp
 from jax import lax
+from jax.experimental import pallas as pl
+from jax.experimental.pallas import tpu as pltpu
 from jax.sharding import PartitionSpec as P
 
 HEAD_DIM = 64
@@ -73,7 +77,356 @@
     return lax.all_to_all(results, "ep", split_axis=0, concat_axis=0, tiled=True)
 
 
-def shards(
+MESH = pl.DeviceIdType.MESH
+TILE = 1024
+
+
+def flip(index, pattern, size):
+    result = 0
+    bit = 1
+    while bit < size:
+        both = lax.rem(lax.div(index, bit) + lax.div(pattern, bit), 2)
+        result = result + both * bit
+        bit = bit * 2
+    return result
+
+
+def fused_kernel(
+    n,
+    laid,
+    q_ref,
+    kv_ref,
+    wg_hbm,
+    wu_hbm,
+    wd_hbm,
+    ow_hbm,
+    back,
+    mixed,
+    wg,
+    wu,
+    wd,
+    ow,
+    rows,
+    partial,
+    red,
+    q_send,
+    x_got,
+    y_send,
+    kv_all,
+    attended,
+    m_part,
+    m_red,
+    m_send,
+    m_got,
+    load_sem,
+    kv_sems,
+    disp_sems,
+    fwd_sems,
+    red_sems,
+    ret_sems,
+    mix_sems,
+):
+    e = lax.axis_index("ep")
+    t = lax.axis_index("tp")
+    side = lax.div(t, 2)
+    core = lax.rem(t, 2)
+    other_side = 1 - side
+    other_core = 1 - core
+    x_peer = (e, other_side * 2 + core)
+    c_peer = (e, side * 2 + other_core)
+    cap, width = laid.shape[1], laid.shape[2]
+    pairs = attended.shape[0]
+    tok = attended.shape[1]
+
+    def remote(src, dst, send, recv, device):
+        return pltpu.make_async_remote_copy(
+            src_ref=src, dst_ref=dst, send_sem=send, recv_sem=recv, device_id=device, device_id_type=MESH
+        )
+
+    loads = [
+        pltpu.make_async_copy(a, b, load_sem.at[k])
+        for k, (a, b) in enumerate([(ow_hbm, ow), (wg_hbm, wg), (wu_hbm, wu), (wd_hbm, wd)])
+    ]
+    for load in loads:
+        load.start()
+
+    barrier = pltpu.get_barrier_semaphore()
+    for s in range(1, n):
+        pl.semaphore_signal(barrier, inc=1, device_id=(flip(e, s, n), t), device_id_type=MESH)
+    pl.semaphore_signal(barrier, inc=1, device_id=x_peer, device_id_type=MESH)
+    pl.semaphore_signal(barrier, inc=1, device_id=c_peer, device_id_type=MESH)
+    pl.semaphore_wait(barrier, n + 1)
+
+    def kv_direct(s):
+        return remote(kv_ref, kv_all.at[:, e], kv_sems.at[0, s], kv_sems.at[1, s], (flip(e, s, n), t))
+
+    def kv_direct_in(s):
+        return remote(kv_ref, kv_all.at[:, flip(e, s, n)], kv_sems.at[0, s], kv_sems.at[1, s], (flip(e, s, n), t))
+
+    def kv_relay(s):
+        owner = flip(e, s, n)
+        return remote(kv_all.at[:, owner], kv_all.at[:, owner], kv_sems.at[0, s + 1], kv_sems.at[1, s + 1], (flip(e, 1, n), t))
+
+    def kv_relay_in(s):
+        owner = flip(e, s + 1, n)
+        return remote(kv_all.at[:, owner], kv_all.at[:, owner], kv_sems.at[0, s + 1], kv_sems.at[1, s + 1], (flip(e, 1, n), t))
+
+    def pattern(i):
+        return jnp.where(i < n // 2, 2 * i, 2 * (n - 1 - i) + 1)
+
+    def dispatch(i):
+        s = pattern(i)
+        return remote(laid.at[flip(e, s, n)], rows.at[e, t], disp_sems.at[0, i], disp_sems.at[1, i], (flip(e, s, n), t))
+
+    def dispatch_in(i):
+        s = pattern(i)
+        return remote(laid.at[flip(e, s, n)], rows.at[flip(e, s, n), t], disp_sems.at[0, i], disp_sems.at[1, i], (flip(e, s, n), t))
+
+    def owner_of(i):
+        return flip(e, pattern(i), n)
+
+    def to_side(i):
+        o = owner_of(i)
+        return remote(rows.at[o, t], rows.at[o, t], fwd_sems.at[0, 0, i], fwd_sems.at[1, 0, i], x_peer)
+
+    def from_side(i):
+        o = owner_of(i)
+        return remote(rows.at[o, t], rows.at[o, other_side * 2 + core], fwd_sems.at[0, 0, i], fwd_sems.at[1, 0, i], x_peer)
+
+    def to_core(i):
+        o = owner_of(i)
+        return remote(rows.at[o, t], rows.at[o, t], fwd_sems.at[0, 1, i], fwd_sems.at[1, 1, i], c_peer)
+
+    def from_core(i):
+        o = owner_of(i)
+        return remote(rows.at[o, t], rows.at[o, side * 2 + other_core], fwd_sems.at[0, 1, i], fwd_sems.at[1, 1, i], c_peer)
+
+    def relay_core(i):
+        o = owner_of(i)
+        slot = other_side * 2 + core
+        return remote(rows.at[o, slot], rows.at[o, slot], fwd_sems.at[0, 2, i], fwd_sems.at[1, 2, i], c_peer)
+
+    def relayed_core(i):
+        o = owner_of(i)
+        slot = other_side * 2 + core
+        return remote(rows.at[o, slot], rows.at[o, other_side * 2 + other_core], fwd_sems.at[0, 2, i], fwd_sems.at[1, 2, i], c_peer)
+
+    def reduce_core(i):
+        return remote(partial.at[i, :, other_core], red.at[i], red_sems.at[0, 0, i], red_sems.at[1, 0, i], c_peer)
+
+    def reduce_side(i):
+        return remote(q_send.at[i], x_got.at[i], red_sems.at[0, 1, i], red_sems.at[1, 1, i], x_peer)
+
+    def give_back(i):
+        o = owner_of(i)
+        return remote(y_send.at[i], back.at[e], ret_sems.at[0, i], ret_sems.at[1, i], (o, t))
+
+    def get_back(i):
+        o = owner_of(i)
+        return remote(y_send.at[i], back.at[o], ret_sems.at[0, i], ret_sems.at[1, i], (o, t))
+
+    mix_core = remote(m_part.at[:, other_core], m_red, mix_sems.at[0, 0], mix_sems.at[1, 0], c_peer)
+    mix_side = remote(m_send, m_got, mix_sems.at[0, 1], mix_sems.at[1, 1], x_peer)
+
+    own = pltpu.make_async_copy(laid.at[e], rows.at[e, t], load_sem.at[4])
+    own_kv = pltpu.make_async_copy(kv_ref, kv_all.at[:, e], load_sem.at[5])
+    own.start()
+    own_kv.start()
+    for s in range(2, n, 2):
+        kv_direct(s).start()
+    kv_direct(1).start()
+    for i in range(1, n):
+        dispatch(i).start()
+    own.wait()
+    to_side(0).start()
+    to_core(0).start()
+    own_kv.wait()
+
+    def attend(pair):
+        kv = kv_all[lax.div(pair * 2 * kv_all.shape[0], pairs * 2)].reshape(n * tok, 128)
+        halves = []
+        for h in range(2):
+            scores = lax.dot_general(
+                q_ref[pair * 2 + h], kv, (((1,), (1,)), ((), ())), preferred_element_type=jnp.float32
+            ) * (HEAD_DIM ** (-0.5))
+            peak = jnp.max(scores, axis=1, keepdims=True)
+            weights = jnp.exp(scores - peak)
+            total = jnp.sum(weights, axis=1, keepdims=True)
+            summed = jnp.dot(weights.astype(jnp.bfloat16), kv, preferred_element_type=jnp.float32)
+            halves.append(summed / total)
+        lane = lax.broadcasted_iota(jnp.int32, halves[0].shape, 1)
+        joined = jnp.where(lane < HEAD_DIM, pltpu.roll(halves[0], HEAD_DIM, 1), halves[1])
+        attended[pair] = joined.astype(jnp.bfloat16)
+
+    def f32(value):
+        return value.astype(jnp.float32)
+
+    def step(i, carry):
+        @pl.when(jnp.logical_and(i > 0, i < n))
+        def _():
+            dispatch_in(i).wait_recv()
+            to_side(i).start()
+            to_core(i).start()
+
+        @pl.when(i == 0)
+        def _():
+            for s in range(2, n, 2):
+                kv_direct_in(s).wait_recv()
+                kv_relay(s).start()
+
+        @pl.when(i == 1)
+        def _():
+            kv_direct_in(1).wait_recv()
+            for s in range(2, n, 2):
+                kv_relay_in(s).wait_recv()
+
+        @pl.when(jnp.logical_and(i >= 1, i <= n))
+        def _():
+            from_side(i - 1).wait_recv()
+            relay_core(i - 1).start()
+
+        @pl.when(jnp.logical_and(i >= 1, i <= pairs))
+        def _():
+            attend(i - 1)
+
+        @pl.when(i == pairs + 1)
+        def _():
+            loads[0].wait()
+            for tile in range(0, width, TILE):
+                product = jnp.dot(attended[0], ow[0, :, tile:tile + TILE], preferred_element_type=jnp.float32)
+                for p in range(1, pairs):
+                    product += jnp.dot(attended[p], ow[p, :, tile:tile + TILE], preferred_element_type=jnp.float32)
+                m_part[:, :, :, tile:tile + TILE] = product.astype(jnp.bfloat16).reshape(2, 2, tok // 4, TILE)
+            mix_core.start()
+
+        @pl.when(i == pairs + 2)
+        def _():
+            mix_core.wait_recv()
+            m_send[...] = (f32(m_part[other_side, core]) + f32(m_red[other_side])).astype(jnp.bfloat16)
+            mix_side.start()
+
+        @pl.when(jnp.logical_and(i >= 2, i < n + 2))
+        def _():
+            k = i - 2
+
+            @pl.when(k == 0)
+            def _():
+                for load in loads[1:]:
+                    load.wait()
+
+            from_core(k).wait_recv()
+            relayed_core(k).wait_recv()
+            tokens = rows[owner_of(k)].reshape(4 * cap, width)
+            gate = jnp.dot(tokens, wg[...], preferred_element_type=jnp.float32)
+            up = jnp.dot(tokens, wu[...], preferred_element_type=jnp.float32)
+            hidden = (gate / (1.0 + jnp.exp(-gate)) * up).astype(jnp.bfloat16)
+            for tile in range(0, width, TILE):
+                product = jnp.dot(hidden, wd[:, tile:tile + TILE], preferred_element_type=jnp.float32)
+                partial[k, :, :, :, tile:tile + TILE] = product.astype(jnp.bfloat16).reshape(2, 2, cap, TILE)
+            reduce_core(k).start()
+
+        @pl.when(jnp.logical_and(i >= 3, i < n + 3))
+        def _():
+            k = i - 3
+            reduce_core(k).wait_recv()
+            q_send[k] = (f32(partial[k, other_side, core]) + f32(red[k, other_side])).astype(jnp.bfloat16)
+            reduce_side(k).start()
+
+        @pl.when(jnp.logical_and(i >= 4, i < n + 4))
+        def _():
+            k = i - 4
+            reduce_side(k).wait_recv()
+            y = (f32(partial[k, side, core]) + f32(red[k, side]) + f32(x_got[k])).astype(jnp.bfloat16)
+
+            @pl.when(k == 0)
+            def _():
+                back[e] = y
+
+            @pl.when(k > 0)
+            def _():
+                y_send[k] = y
+                give_back(k).start()
+
+        return carry
+
+    lax.fori_loop(0, n + 4, step, 0)
+
+    mix_side.wait_recv()
+    mixed[...] = (f32(m_part[side, core]) + f32(m_red[side]) + f32(m_got[...])).astype(jnp.bfloat16)
+    mix_core.wait_send()
+    mix_side.wait_send()
+    for s in range(2, n, 2):
+        kv_direct(s).wait_send()
+        kv_relay(s).wait_send()
+    kv_direct(1).wait_send()
+
+    def drain(i, carry):
+        @pl.when(i > 0)
+        def _():
+            dispatch(i).wait_send()
+            give_back(i).wait_send()
+            get_back(i).wait_recv()
+
+        to_side(i).wait_send()
+        to_core(i).wait_send()
+        relay_core(i).wait_send()
+        reduce_core(i).wait_send()
+        reduce_side(i).wait_send()
+        return carry
+
+    lax.fori_loop(0, n, drain, 0)
+
+
+def fused(laid, q_heads, kv_pack, gate_weight, up_weight, down_weight, out_weight):
+    n, cap, width = laid.shape
+    heads, tok, _ = q_heads.shape
+    kv_count = kv_pack.shape[0]
+    pairs = heads // 2
+    hidden = gate_weight.shape[1]
+    bf = jnp.bfloat16
+    vmem = pl.BlockSpec(memory_space=pltpu.VMEM)
+    anywhere = pl.BlockSpec(memory_space=pl.ANY)
+    dma = pltpu.SemaphoreType.DMA
+    return pl.pallas_call(
+        functools.partial(fused_kernel, n),
+        out_shape=(
+            jax.ShapeDtypeStruct((n, cap, width), bf),
+            jax.ShapeDtypeStruct((tok // 4, width), bf),
+        ),
+        in_specs=[vmem] * 3 + [anywhere] * 4,
+        out_specs=(vmem, vmem),
+        scratch_shapes=[
+            pltpu.VMEM((width, hidden), bf),
+            pltpu.VMEM((width, hidden), bf),
+            pltpu.VMEM((hidden, width), bf),
+            pltpu.VMEM((pairs, 128, width), bf),
+            pltpu.VMEM((n, 4, cap, width), bf),
+            pltpu.VMEM((n, 2, 2, cap, width), bf),
+            pltpu.VMEM((n, 2, cap, width), bf),
+            pltpu.VMEM((n, cap, width), bf),
+            pltpu.VMEM((n, cap, width), bf),
+            pltpu.VMEM((n, cap, width), bf),
+            pltpu.VMEM((kv_count, n, tok, 128), bf),
+            pltpu.VMEM((pairs, tok, 128), bf),
+            pltpu.VMEM((2, 2, tok // 4, width), bf),
+            pltpu.VMEM((2, tok // 4, width), bf),
+            pltpu.VMEM((tok // 4, width), bf),
+            pltpu.VMEM((tok // 4, width), bf),
+            dma((6,)),
+            dma((2, n)),
+            dma((2, n)),
+            dma((2, 3, n)),
+            dma((2, 2, n)),
+            dma((2, n)),
+            dma((2, 2)),
+        ],
+        compiler_params=pltpu.CompilerParams(
+            collective_id=0, has_side_effects=True, vmem_limit_bytes=62 * 1024 * 1024
+        ),
+    )(laid, q_heads, kv_pack, gate_weight, up_weight, down_weight, out_weight.reshape(pairs, 128, width))
+
+
+def plain_shards(
     queries,
     keys,
     values,
@@ -179,6 +532,87 @@
     return (mixed, moe_out)
 
 
+def shards(
+    queries,
+    keys,
+    values,
+    query_gain,
+    key_gain,
+    out_weight,
+    expert_input,
+    norm_gain,
+    routes,
+    route_weight,
+    gate_weight,
+    up_weight,
+    down_weight,
+):
+    tok_exp, model_width = expert_input.shape
+    top_count = routes.shape[1]
+    expert_count = lax.axis_size("ep")
+    capacity = 2 * top_count * tok_exp // expert_count
+    if capacity % 16 != 0 or lax.axis_size("tp") != 4:
+        return plain_shards(
+            queries,
+            keys,
+            values,
+            query_gain,
+            key_gain,
+            out_weight,
+            expert_input,
+            norm_gain,
+            routes,
+            route_weight,
+            gate_weight,
+            up_weight,
+            down_weight,
+        )
+    tok_mix = queries.shape[0]
+    head_count = query_gain.shape[0] // HEAD_DIM
+    kv_count = key_gain.shape[0] // HEAD_DIM
+    offset = lax.axis_index("ep") * tok_mix
+    q_turned = head_norm(queries, query_gain, head_count, offset)
+    k_turned = head_norm(keys, key_gain, kv_count, offset)
+    q_heads = jnp.transpose(q_turned.reshape(tok_mix, head_count, HEAD_DIM), (1, 0, 2))
+    q_heads = jnp.pad(q_heads, ((0, 0), (0, 0), (0, HEAD_DIM)))
+    kv_pack = jnp.concatenate(
+        [k_turned.reshape(tok_mix, kv_count, HEAD_DIM), values.reshape(tok_mix, kv_count, HEAD_DIM)],
+        axis=-1,
+    )
+    kv_pack = jnp.transpose(kv_pack, (1, 0, 2))
+    as_float = expert_input.astype(jnp.float32)
+    normed = (
+        as_float
+        * lax.rsqrt(jnp.mean(as_float * as_float, axis=-1, keepdims=True) + NORM_EPS)
+        * norm_gain
+    ).astype(jnp.bfloat16)
+    flat_routes = routes.reshape(-1)
+    route_hits = (
+        flat_routes[:, None] == jnp.arange(expert_count, dtype=jnp.int32)[None, :]
+    ).astype(jnp.int32)
+    slot_rank = jnp.sum((jnp.cumsum(route_hits, axis=0) - route_hits) * route_hits, axis=1)
+    slot_ids = (flat_routes * capacity + slot_rank).reshape(tok_exp, top_count)
+    slots = jnp.arange(expert_count * capacity, dtype=jnp.int32)
+    placed = jnp.any(slots[:, None, None] == slot_ids[None], axis=2).astype(jnp.bfloat16)
+    outbound = jnp.dot(placed, normed, preferred_element_type=jnp.float32).astype(jnp.bfloat16)
+    back_rows, mixed = fused(
+        outbound.reshape(expert_count, capacity, model_width),
+        q_heads,
+        kv_pack,
+        gate_weight[0],
+        up_weight[0],
+        down_weight[0],
+        out_weight,
+    )
+    back_rows = back_rows.reshape(expert_count * capacity, model_width)
+    moe_sum = jnp.zeros((tok_exp, model_width), jnp.float32)
+    for k in range(top_count):
+        chosen = (slot_ids[:, k, None] == slots[None, :]).astype(jnp.bfloat16)
+        picked = jnp.dot(chosen, back_rows, preferred_element_type=jnp.float32)
+        moe_sum = moe_sum + picked * route_weight[:, k, None]
+    return (mixed, moe_sum.astype(jnp.bfloat16))
+
+
 def solution(mesh):
     placed = (
         P("ep", "tp"),

time: 271 us -> 167 us (0.62)
  Pallas kernels: 0 us -> 149 us
  blocking collectives: 135 us -> 0 us
  waiting for transfers between devices: 45.4 us -> 0 us
  matrix products: 38.4 us -> 5.72 us
  between operations: 14.1 us -> 0.9 us
  starting transfers between devices: 10.1 us -> 0 us
  local copies, waits for them, and re-layouts: 13.5 us -> 4.57 us
  other arithmetic: 14.4 us -> 6.7 us
    pallas_call x0 -> x1, Pallas kernels: none -> 149 us  [fused(): pl.pallas_call(functools.partial(fused_kernel, n), out_shape=(jax.ShapeDt...]
    all_gather x2 -> x0, blocking collectives: 72.9 us -> none  [the longest x1 41.5 us: shards(): value_piece = lax.all_gather(values, 'ep', axis=0, tiled=True)]
    all_to_all x2 -> x0, blocking collectives: 61.9 us -> none  [run_experts(): lax.all_to_all(sending, 'ep', split_axis=0, concat_axis=0, tiled=True)]
    dot_general x7 -> x2, matrix products: 36.6 us -> 3.58 us  [shards(): picked = jnp.dot(chosen, back_rows, preferred_element_type=jnp.float32)]
    all_gather x2 -> x0, waiting for transfers between devices: 27 us -> none  [run_experts(): shard_rows = lax.all_gather(arrived, 'tp', axis=0, tiled=True)]
    all_to_all x2 -> x0, waiting for transfers between devices: 18.3 us -> none  [run_experts(): lax.all_to_all(results, 'ep', split_axis=0, concat_axis=0, tiled=True)]
    all_to_all x2 -> x0, starting transfers between devices: 9.9 us -> none  [run_experts(): lax.all_to_all(results, 'ep', split_axis=0, concat_axis=0, tiled=True)]
    reduce_sum x2 -> x0, other arithmetic: 7.27 us -> none  [the longest x1 5.55 us: shards(): jnp.sum(picked.astype(jnp.float32) * route_weight[:, :, None], axis=1)]
  transfers between devices with their start and end apart: 7 -> 0, of which waited for: 3 -> 0; matrix products, arithmetic and copies ran while one was open for 21% -> 0% of each run, Pallas kernels for 0% -> 0%
where the time goes in v1:
time: 167 us
  Pallas kernels  149 us (89%)
  other arithmetic  6.7 us (4%)
  matrix products  5.72 us (3%)
  local copies, waits for them, and re-layouts  4.57 us (3%)
    pallas_call x1, Pallas kernels, fused(): pl.pallas_call(functools.partial(fused_kernel, n), out_shape=(jax.ShapeDt...  149 us
    dot_general x2, matrix products, shards(): picked = jnp.dot(chosen, back_rows, preferred_element_type=jnp.float32)  3.58 us

profile of v1, /device:TPU:0, one launch (start us, length us, event | category | flops | bytes accessed | tf_op | source)
XLA Modules:
  0.0 167.1 jit_solution(14333488782724502284)
XLA Ops:
  0.6 1.1 copy.39
  1.7 0.2 copy.40
  1.9 0.1 multiply_reduce_fusion
  2.0 0.8 mul.189
  2.7 0.3 multiply_multiply_fusion
  3.0 1.5 slice_negate_fusion.1
  4.6 0.1 broadcast_multiply_fusion.1
  4.7 0.5 fusion.18
  5.2 0.0 copy-start.3
  5.2 0.0 copy-start.8
  5.2 2.0 %fusion.10 = bf16[8,192,64]{2,1,0:T(8,128)(2,1)S(1)} fusion(f32[192,64]{1,0:T(8,128)S(1)} %get-tuple-element.15, f32[192,8,16]{2,0,1:T(8,128)S(1)} %get-tuple-element.7, f32[192,8,16]{2,0,1:T(8,128)S(1)} %get-tuple-element.8, f32[192,8,16]{2,0,1:T(8,128)} %get-tuple-element.9, f32[192,8,16]{2,0,1:T(8,128)S(1)} %get-tuple-element.6, ...), kind=kLoop, calls=%fused_computation.19 | loop fusion | flops 884736 | bytes 1089536 | tf_op jit(solution)/shard_map/transpose | solution.py:576
  7.2 0.0 copy-start.4
  7.2 0.8 pad.4.q_ref
  8.1 0.0 copy-done.3
  8.1 0.1 copy.41
  8.2 0.0 copy-start.6
  8.2 0.1 copy.42
  8.4 0.0 copy-done.8
  8.4 0.1 mul.205
  8.4 0.1 multiply_multiply_fusion.1
  8.6 0.0 copy-start.5
  8.6 0.2 slice_negate_fusion.3
  8.8 0.3 fusion.12
  9.1 0.0 copy-done.4
  9.1 0.1 copy.43
  9.2 0.1 copy.44
  9.3 0.7 maximum_bitcast_fusion.kv_ref
  10.1 0.0 copy-done.6
  10.1 0.1 copy.37
  10.2 0.1 eq.62
  10.3 0.1 fusion.14
  10.4 0.2 reduce_window_sum.11
  10.6 0.2 select_reduce_fusion
  10.8 0.1 reduce_sum.39
  10.9 0.1 copy.38
  11.0 0.1 fusion.13
  11.1 0.0 copy-done.1
  11.1 0.2 fusion.2
  11.3 0.0 copy-done.5
  11.3 2.1 %convolution_convert_fusion = bf16[256,4096]{1,0:T(8,128)(2,1)} fusion(pred[256,64]{0,1:T(8,128)(4,1)S(1)} %fusion.13, bf16[64,4096]{1,0:T(8,128)(2,1)S(1)} %copy-done.1, f32[4096]{0:T(1024)S(1)} %copy-done.5, f32[64]{0:T(128)S(1)} %add_rsqrt_fusion.2), kind=kOutput, calls=%fused_computation | convolution fusion | flops 136314880 | bytes 2654464 | tf_op jit(solution)/shard_map/dot_general | solution.py:597
  13.5 149.2 %shard_map.140 = (bf16[8,32,4096]{2,1,0:T(8,128)(2,1)}, bf16[48,4096]{1,0:T(8,128)(2,1)}) custom-call(bf16[8,32,4096]{2,1,0:T(8,128)(2,1)} %bitcast.28, bf16[8,192,128]{2,1,0:T(8,128)(2,1)} %pad.4.q_ref, bf16[2,192,128]{2,1,0:T(8,128)(2,1)} %maximum_bitcast_fusion.kv_ref, bf16[4096,256]{1,0:T(8,128)(2,1)} %bitcast.33, bf16[4096,256]{1,0:T(8,128)(2,1)} %bitcast.34, ...), custom_call_target="tpu_custom_call" | custom-call | tf_op jit(solution)/shard_map/pallas_call | solution.py:390
  162.7 0.0 copy-start
  162.7 0.0 copy-done.7
  162.7 2.3 %convolution_multiply_fusion.1 = f32[64,4096]{1,0:T(8,128)S(1)} fusion(bf16[256,4096]{1,0:T(8,128)(2,1)} %bitcast.29, f32[64]{0:T(128)S(1)} %get-tuple-element.19, s32[64]{0:T(128)S(1)} %get-tuple-element.17), kind=kOutput, calls=%fused_computation.3 | convolution fusion | flops 134496256 | bytes 3146240 | tf_op jit(solution)/shard_map/dot_general | solution.py:611
  165.0 0.0 copy-start.2
  165.0 0.0 copy-done
  165.0 1.3 fusion.1
  166.3 0.7 copy.46
  (12 shorter events, 0.1 us)
Async XLA Ops:
  5.2 2.9 %copy-start.3 = (bf16[192,128]{1,0:T(8,128)(2,1)S(1)}, bf16[192,128]{1,0:T(8,128)(2,1)}, u32[]{:S(2)}) copy-start(bf16[192,128]{1,0:T(8,128)(2,1)} %param.14) | copy-start | bytes 147460
  5.2 3.2 %copy-start.8 = (f32[128]{0:T(128)S(1)}, f32[128]{0:T(128)}, u32[]{:S(2)}) copy-start(f32[128]{0:T(128)} %param.17) | copy-start | bytes 1540
  7.2 1.9 %copy-start.4 = (bf16[192,128]{1,0:T(8,128)(2,1)S(1)}, bf16[192,128]{1,0:T(8,128)(2,1)}, u32[]{:S(2)}) copy-start(bf16[192,128]{1,0:T(8,128)(2,1)} %param.15) | copy-start | bytes 147460
  8.2 1.9 %copy-start.6 = (s32[64,2]{0,1:T(2,128)S(1)}, s32[64,2]{0,1:T(2,128)}, u32[]{:S(2)}) copy-start(s32[64,2]{0,1:T(2,128)} %param.21) | copy-start | bytes 1540
  8.4 2.7 %copy-start.1 = (bf16[64,4096]{1,0:T(8,128)(2,1)S(1)}, bf16[64,4096]{1,0:T(8,128)(2,1)}, u32[]{:S(2)}) copy-start(bf16[64,4096]{1,0:T(8,128)(2,1)} %param.19) | copy-start | bytes 1572868
  8.6 2.8 %copy-start.5 = (f32[4096]{0:T(1024)S(1)}, f32[4096]{0:T(1024)}, u32[]{:S(2)}) copy-start(f32[4096]{0:T(1024)} %param.20) | copy-start | bytes 49156
  13.5 149.2 %copy-start.7 = (f32[64,2]{0,1:T(2,128)S(1)}, f32[64,2]{0,1:T(2,128)}, u32[]{:S(2)}) copy-start(f32[64,2]{0,1:T(2,128)} %param.22) | copy-start | bytes 1540
  162.7 2.3 %copy-start = (bf16[8,32,4096]{2,1,0:T(8,128)(2,1)S(1)}, bf16[8,32,4096]{2,1,0:T(8,128)(2,1)}, u32[]{:S(2)}) copy-start(bf16[8,32,4096]{2,1,0:T(8,128)(2,1)} %get-tuple-element.5) | copy-start | bytes 6291460
  165.0 1.3 copy-start.2

commit v2 on v1

--- a/solution.py
+++ b/solution.py
@@ -171,8 +171,13 @@
         owner = flip(e, s + 1, n)
         return remote(kv_all.at[:, owner], kv_all.at[:, owner], kv_sems.at[0, s + 1], kv_sems.at[1, s + 1], (flip(e, 1, n), t))
 
+    order = [0, 1] + sorted(range(2, n), key=lambda s: (s < 4, s % 2, -s))
+
     def pattern(i):
-        return jnp.where(i < n // 2, 2 * i, 2 * (n - 1 - i) + 1)
+        chosen = order[0]
+        for place in range(1, n):
+            chosen = jnp.where(i == place, order[place], chosen)
+        return chosen
 
     def dispatch(i):
         s = pattern(i)
@@ -232,11 +237,15 @@
     own_kv = pltpu.make_async_copy(kv_ref, kv_all.at[:, e], load_sem.at[5])
     own.start()
     own_kv.start()
+    for i in range(1, n):
+        if i == 8:
+            for s in range(2, n, 2):
+                kv_direct(s).start()
+            kv_direct(1).start()
+        dispatch(i).start()
     for s in range(2, n, 2):
         kv_direct(s).start()
     kv_direct(1).start()
-    for i in range(1, n):
-        dispatch(i).start()
     own.wait()
     to_side(0).start()
     to_core(0).start()
@@ -268,28 +277,29 @@
             to_side(i).start()
             to_core(i).start()
 
-        @pl.when(i == 0)
+        @pl.when(i == 6)
         def _():
             for s in range(2, n, 2):
                 kv_direct_in(s).wait_recv()
                 kv_relay(s).start()
 
-        @pl.when(i == 1)
+        @pl.when(jnp.logical_and(i >= 1, i <= n))
+        def _():
+            from_side(i - 1).wait_recv()
+            relay_core(i - 1).start()
+
+        @pl.when(i == 7)
         def _():
             kv_direct_in(1).wait_recv()
             for s in range(2, n, 2):
                 kv_relay_in(s).wait_recv()
 
-        @pl.when(jnp.logical_and(i >= 1, i <= n))
-        def _():
-            from_side(i - 1).wait_recv()
-            relay_core(i - 1).start()
-
-        @pl.when(jnp.logical_and(i >= 1, i <= pairs))
-        def _():
-            attend(i - 1)
-
-        @pl.when(i == pairs + 1)
+        @pl.when(jnp.logical_and(i >= 7, i < 7 + pairs // 2))
+        def _():
+            attend(2 * (i - 7))
+            attend(2 * (i - 7) + 1)
+
+        @pl.when(i == 7 + pairs // 2)
         def _():
             loads[0].wait()
             for tile in range(0, width, TILE):
@@ -299,15 +309,9 @@
                 m_part[:, :, :, tile:tile + TILE] = product.astype(jnp.bfloat16).reshape(2, 2, tok // 4, TILE)
             mix_core.start()
 
-        @pl.when(i == pairs + 2)
-        def _():
-            mix_core.wait_recv()
-            m_send[...] = (f32(m_part[other_side, core]) + f32(m_red[other_side])).astype(jnp.bfloat16)
-            mix_side.start()
-
-        @pl.when(jnp.logical_and(i >= 2, i < n + 2))
-        def _():
-            k = i - 2
+        @pl.when(jnp.logical_and(i >= 1, i <= n))
+        def _():
+            k = i - 1
 
             @pl.when(k == 0)
             def _():
@@ -325,16 +329,15 @@
                 partial[k, :, :, :, tile:tile + TILE] = product.astype(jnp.bfloat16).reshape(2, 2, cap, TILE)
             reduce_core(k).start()
 
-        @pl.when(jnp.logical_and(i >= 3, i < n + 3))
-        def _():
-            k = i - 3
-            reduce_core(k).wait_recv()
-            q_send[k] = (f32(partial[k, other_side, core]) + f32(red[k, other_side])).astype(jnp.bfloat16)
-            reduce_side(k).start()
-
-        @pl.when(jnp.logical_and(i >= 4, i < n + 4))
-        def _():
-            k = i - 4
+        @pl.when(i == 7 + pairs // 2)
+        def _():
+            mix_core.wait_recv()
+            m_send[...] = (f32(m_part[other_side, core]) + f32(m_red[other_side])).astype(jnp.bfloat16)
+            mix_side.start()
+
+        @pl.when(jnp.logical_and(i >= 2, i < n + 2))
+        def _():
+            k = i - 2
             reduce_side(k).wait_recv()
             y = (f32(partial[k, side, core]) + f32(red[k, side]) + f32(x_got[k])).astype(jnp.bfloat16)
 
@@ -347,9 +350,16 @@
                 y_send[k] = y
                 give_back(k).start()
 
+        @pl.when(jnp.logical_and(i >= 1, i <= n))
+        def _():
+            k = i - 1
+            reduce_core(k).wait_recv()
+            q_send[k] = (f32(partial[k, other_side, core]) + f32(red[k, other_side])).astype(jnp.bfloat16)
+            reduce_side(k).start()
+
         return carry
 
-    lax.fori_loop(0, n + 4, step, 0)
+    lax.fori_loop(0, n + 2, step, 0)
 
     mix_side.wait_recv()
     mixed[...] = (f32(m_part[side, core]) + f32(m_red[side]) + f32(m_got[...])).astype(jnp.bfloat16)

time: 167 us -> 141 us (0.84)
  Pallas kernels: 149 us -> 123 us
    pallas_call x1, Pallas kernels: 149 us -> 123 us  [fused(): pl.pallas_call(functools.partial(fused_kernel, n), out_shape=(jax.ShapeDt...]
where the time goes in v2:
time: 141 us
  Pallas kernels  123 us (87%)
  other arithmetic  6.7 us (5%)
  matrix products  5.71 us (4%)
  local copies, waits for them, and re-layouts  4.57 us (3%)
    pallas_call x1, Pallas kernels, fused(): pl.pallas_call(functools.partial(fused_kernel, n), out_shape=(jax.ShapeDt...  123 us
    dot_general x2, matrix products, shards(): picked = jnp.dot(chosen, back_rows, preferred_element_type=jnp.float32)  3.58 us

profile of v2, /device:TPU:0, one launch (start us, length us, event | category | flops | bytes accessed | tf_op | source)
XLA Modules:
  0.0 141.3 jit_solution(12294142639285014405)
XLA Ops:
  0.6 1.1 copy.39
  1.7 0.2 copy.40
  1.9 0.1 multiply_reduce_fusion
  2.0 0.8 mul.189
  2.7 0.3 multiply_multiply_fusion
  3.0 1.5 %slice_negate_fusion.1 = (f32[192,8,16]{2,0,1:T(8,128)S(1)}, f32[192,8,16]{2,0,1:T(8,128)S(1)}, f32[192,8,16]{2,0,1:T(8,128)S(1)}, f32[192,8,16]{2,0,1:T(8,128)}) fusion(f32[192,8,64]{2,0,1:T(8,128)S(1)} %multiply_multiply_fusion), kind=kLoop, calls=%fused_computation.11 | loop fusion | flops 49152 | bytes 786432 | tf_op jit(solution)/shard_map/neg | solution.py:25
  4.6 0.1 broadcast_multiply_fusion.1
  4.7 0.5 fusion.18
  5.2 0.0 copy-start.3
  5.2 0.0 copy-start.8
  5.2 2.0 %fusion.10 = bf16[8,192,64]{2,1,0:T(8,128)(2,1)S(1)} fusion(f32[192,64]{1,0:T(8,128)S(1)} %get-tuple-element.15, f32[192,8,16]{2,0,1:T(8,128)S(1)} %get-tuple-element.7, f32[192,8,16]{2,0,1:T(8,128)S(1)} %get-tuple-element.8, f32[192,8,16]{2,0,1:T(8,128)} %get-tuple-element.9, f32[192,8,16]{2,0,1:T(8,128)S(1)} %get-tuple-element.6, ...), kind=kLoop, calls=%fused_computation.19 | loop fusion | flops 884736 | bytes 1089536 | tf_op jit(solution)/shard_map/transpose | solution.py:586
  7.2 0.0 copy-start.4
  7.2 0.8 pad.4.q_ref
  8.1 0.0 copy-done.3
  8.1 0.1 copy.41
  8.2 0.0 copy-start.6
  8.2 0.1 copy.42
  8.4 0.0 copy-done.8
  8.4 0.1 mul.205
  8.4 0.1 multiply_multiply_fusion.1
  8.6 0.0 copy-start.5
  8.6 0.2 slice_negate_fusion.3
  8.8 0.3 fusion.12
  9.1 0.0 copy-done.4
  9.1 0.1 copy.43
  9.2 0.1 copy.44
  9.3 0.7 maximum_bitcast_fusion.kv_ref
  10.1 0.0 copy-done.6
  10.1 0.1 copy.37
  10.2 0.1 eq.62
  10.3 0.1 fusion.14
  10.4 0.2 reduce_window_sum.11
  10.6 0.2 select_reduce_fusion
  10.8 0.1 reduce_sum.39
  10.9 0.1 copy.38
  11.0 0.1 fusion.13
  11.1 0.0 copy-done.1
  11.1 0.2 fusion.2
  11.3 0.0 copy-done.5
  11.3 2.1 %convolution_convert_fusion = bf16[256,4096]{1,0:T(8,128)(2,1)} fusion(pred[256,64]{0,1:T(8,128)(4,1)S(1)} %fusion.13, bf16[64,4096]{1,0:T(8,128)(2,1)S(1)} %copy-done.1, f32[4096]{0:T(1024)S(1)} %copy-done.5, f32[64]{0:T(128)S(1)} %add_rsqrt_fusion.2), kind=kOutput, calls=%fused_computation | convolution fusion | flops 136314880 | bytes 2654464 | tf_op jit(solution)/shard_map/dot_general | solution.py:607
  13.5 123.4 %shard_map.140 = (bf16[8,32,4096]{2,1,0:T(8,128)(2,1)}, bf16[48,4096]{1,0:T(8,128)(2,1)}) custom-call(bf16[8,32,4096]{2,1,0:T(8,128)(2,1)} %bitcast.28, bf16[8,192,128]{2,1,0:T(8,128)(2,1)} %pad.4.q_ref, bf16[2,192,128]{2,1,0:T(8,128)(2,1)} %maximum_bitcast_fusion.kv_ref, bf16[4096,256]{1,0:T(8,128)(2,1)} %bitcast.33, bf16[4096,256]{1,0:T(8,128)(2,1)} %bitcast.34, ...), custom_call_target="tpu_custom_call" | custom-call | tf_op jit(solution)/shard_map/pallas_call | solution.py:400
  136.9 0.0 copy-start
  136.9 0.0 copy-done.7
  136.9 2.3 %convolution_multiply_fusion.1 = f32[64,4096]{1,0:T(8,128)S(1)} fusion(bf16[256,4096]{1,0:T(8,128)(2,1)} %bitcast.29, f32[64]{0:T(128)S(1)} %get-tuple-element.19, s32[64]{0:T(128)S(1)} %get-tuple-element.17), kind=kOutput, calls=%fused_computation.3 | convolution fusion | flops 134496256 | bytes 3146240 | tf_op jit(solution)/shard_map/dot_general | solution.py:621
  139.2 0.0 copy-start.2
  139.2 0.0 copy-done
  139.2 1.3 fusion.1
  140.5 0.7 copy.46
  (12 shorter events, 0.1 us)
Async XLA Ops:
  5.2 2.9 %copy-start.3 = (bf16[192,128]{1,0:T(8,128)(2,1)S(1)}, bf16[192,128]{1,0:T(8,128)(2,1)}, u32[]{:S(2)}) copy-start(bf16[192,128]{1,0:T(8,128)(2,1)} %param.14) | copy-start | bytes 147460
  5.2 3.2 %copy-start.8 = (f32[128]{0:T(128)S(1)}, f32[128]{0:T(128)}, u32[]{:S(2)}) copy-start(f32[128]{0:T(128)} %param.17) | copy-start | bytes 1540
  7.2 1.9 %copy-start.4 = (bf16[192,128]{1,0:T(8,128)(2,1)S(1)}, bf16[192,128]{1,0:T(8,128)(2,1)}, u32[]{:S(2)}) copy-start(bf16[192,128]{1,0:T(8,128)(2,1)} %param.15) | copy-start | bytes 147460
  8.2 1.9 %copy-start.6 = (s32[64,2]{0,1:T(2,128)S(1)}, s32[64,2]{0,1:T(2,128)}, u32[]{:S(2)}) copy-start(s32[64,2]{0,1:T(2,128)} %param.21) | copy-start | bytes 1540
  8.4 2.7 %copy-start.1 = (bf16[64,4096]{1,0:T(8,128)(2,1)S(1)}, bf16[64,4096]{1,0:T(8,128)(2,1)}, u32[]{:S(2)}) copy-start(bf16[64,4096]{1,0:T(8,128)(2,1)} %param.19) | copy-start | bytes 1572868
  8.6 2.8 %copy-start.5 = (f32[4096]{0:T(1024)S(1)}, f32[4096]{0:T(1024)}, u32[]{:S(2)}) copy-start(f32[4096]{0:T(1024)} %param.20) | copy-start | bytes 49156
  13.5 123.4 %copy-start.7 = (f32[64,2]{0,1:T(2,128)S(1)}, f32[64,2]{0,1:T(2,128)}, u32[]{:S(2)}) copy-start(f32[64,2]{0,1:T(2,128)} %param.22) | copy-start | bytes 1540
  136.9 2.3 %copy-start = (bf16[8,32,4096]{2,1,0:T(8,128)(2,1)S(1)}, bf16[8,32,4096]{2,1,0:T(8,128)(2,1)}, u32[]{:S(2)}) copy-start(bf16[8,32,4096]{2,1,0:T(8,128)(2,1)} %get-tuple-element.5) | copy-start | bytes 6291460
  139.2 1.3 copy-start.2
